TPU v7x, 32 devices: a whole 2x2x4 slice. The times are simulated.
32 devices in a mesh: sp: 8 (over z, x), tp: 4 (over y, core).
Axes of the slice: x: 2, y: 2, z: 4, core: 2. Of those that a mesh axis runs over, the one named last changes fastest.
Arguments:
- residual: bfloat16 [1024, 2048], P('sp'), may hold values from -6 to 6
- queries: bfloat16 [1024, 2048], P('sp', 'tp'), may hold values from -6 to 6
- keys: bfloat16 [1024, 2048], P('sp', 'tp'), may hold values from -6 to 6
- values: bfloat16 [1024, 2048], P('sp', 'tp'), may hold values from -24 to 24
- stick_bias: bfloat16 [32, 1024], P('tp', 'sp'), may hold values from 2 to 13
- query_gain: float32 [64], replicated, may hold values from 0.1 to 1.9
- key_gain: float32 [64], replicated, may hold values from 0.1 to 1.9
- out_weight: bfloat16 [2048, 2048], P('tp'), may hold values from -0.25 to 0.25
- norm_gain: float32 [2048], replicated, may hold values from 0.1 to 1.9
- route_ids: int32 [1024, 2], P('sp'), may hold values from 0 to 7, all different within a row; in each aligned block of 128 rows (0 to 127, 128 to 255, ...) at most 40 rows name the same one
- route_weights: float32 [1024, 2], P('sp'), may hold values from 0.1 to 1
- gate_weight: bfloat16 [8, 2048, 2048], P('sp', None, 'tp'), may hold values from -3 to 3
- up_weight: bfloat16 [8, 2048, 2048], P('sp', None, 'tp'), may hold values from -3 to 3
- down_weight: bfloat16 [8, 2048, 2048], P('sp', 'tp'), may hold values from -0.125 to 0.125
Outputs:
- layer_out: bfloat16 [1024, 2048], P('sp', 'tp')
Inputs may be any that keep to these rules, and one draw needn't show every extreme that they name: `route_ids`: each row names 2 different experts. In every aligned block of 128 rows at most 40 rows name one expert, and in every draw some expert is named by exactly 40 rows of some block.
All inputs are finite; a program needn't handle non-finite values.
Results may differ from a plain program's by a relative error of at most 0.028.
Values may be sent and summed in bfloat16 or wider, within the bound.
A program may use at most 64 MiB of HBM per device.

v0:
```python
import math
import jax
import jax.numpy as jnp
from jax import lax
from jax.sharding import PartitionSpec as P

epsilon = 1e-06
clamp_limit = 7.0
swish_scale = 1.702


def head_normalize(packed, gain):
    values_f = packed.astype(jnp.float32).reshape(packed.shape[0], -1, gain.shape[0])
    scaled = (
        values_f * lax.rsqrt(jnp.mean(values_f * values_f, axis=-1, keepdims=True) + epsilon) * gain
    )
    return scaled.astype(jnp.bfloat16)


def activate(gate_pre, up_pre):
    gate_top = jnp.minimum(gate_pre, clamp_limit)
    up_clip = jnp.clip(up_pre, -clamp_limit, clamp_limit)
    return (up_clip + 1.0) * (gate_top * jax.nn.sigmoid(swish_scale * gate_top))


def slot_table(picked, expert_count, capacity):
    flat_ids = picked.reshape(-1)
    one_hot = (flat_ids[:, None] == jnp.arange(expert_count, dtype=jnp.int32)[None, :]).astype(
        jnp.int32
    )
    before = jnp.sum((jnp.cumsum(one_hot, axis=0) - one_hot) * one_hot, axis=1)
    return flat_ids * capacity + before


def key_block(state_pair, queries_n, keys_block, values_block, bias_block, first_key, query_pos):
    summed, log_carry = state_pair
    key_count = bias_block.shape[1]
    head_total = bias_block.shape[0]
    keys_heads = keys_block.reshape(key_count, head_total, -1)
    values_heads = values_block.reshape(key_count, head_total, -1)
    head_dim = keys_heads.shape[2]
    scores = jnp.einsum(
        "qhd,khd->hqk", queries_n, keys_heads, preferred_element_type=jnp.float32
    ) * head_dim ** (-0.5)
    scores = scores - bias_block.astype(jnp.float32)[:, None, :]
    key_pos = first_key + jnp.arange(key_count, dtype=jnp.int32)
    causal = ((key_pos[None, :] < query_pos[:, None]) & (key_pos[None, :] >= 0))[None]
    log_stay = jnp.where(causal, jax.nn.log_sigmoid(-scores), 0.0)
    later_sum = lax.cumsum(log_stay, axis=2, reverse=True) - log_stay
    weight = jnp.where(
        causal, jnp.exp(jax.nn.log_sigmoid(scores) + later_sum + log_carry[:, :, None]), 0.0
    )
    summed = summed + jnp.einsum(
        "hqk,khd->qhd",
        weight.astype(jnp.bfloat16),
        values_heads,
        preferred_element_type=jnp.float32,
    )
    return (summed, log_carry + jnp.sum(log_stay, axis=2))


def per_device(
    residual,
    queries,
    keys,
    values,
    stick_bias,
    query_gain,
    key_gain,
    out_weight,
    norm_gain,
    route_ids,
    route_weights,
    gate_weight,
    up_weight,
    down_weight,
):
    tok_rows = queries.shape[0]
    width_sp = lax.axis_size("sp")
    offset = lax.axis_index("sp") * tok_rows
    query_pos = offset + jnp.arange(tok_rows, dtype=jnp.int32)
    queries_n = head_normalize(queries, query_gain)
    keys_n = head_normalize(keys, key_gain).reshape(tok_rows, -1)
    head_total = stick_bias.shape[0]
    head_dim = query_gain.shape[0]
    state_pair = (
        jnp.zeros((tok_rows, head_total, head_dim), jnp.float32),
        jnp.zeros((head_total, tok_rows), jnp.float32),
    )
    all_keys, all_values, all_bias = (
        lax.all_gather(keys_n, "sp", axis=0, tiled=True),
        lax.all_gather(values, "sp", axis=0, tiled=True),
        lax.all_gather(stick_bias, "sp", axis=1, tiled=True),
    )
    key_total = all_keys.shape[0]
    block_len = math.gcd(key_total, 512)
    block_total = key_total // block_len

    def sweep_block(block_step, running):
        first_key = (block_total - 1 - block_step) * block_len
        return key_block(
            running,
            queries_n,
            lax.dynamic_slice_in_dim(all_keys, first_key, block_len, 0),
            lax.dynamic_slice_in_dim(all_values, first_key, block_len, 0),
            lax.dynamic_slice_in_dim(all_bias, first_key, block_len, 1),
            first_key,
            query_pos,
        )

    state_pair = lax.fori_loop(0, block_total, sweep_block, state_pair)
    attended = state_pair[0].reshape(tok_rows, head_total * head_dim).astype(jnp.bfloat16)
    partial_value = jnp.dot(attended, out_weight, preferred_element_type=jnp.float32)
    model_width = residual.shape[1]
    expert_count = width_sp * gate_weight.shape[0]
    pick_count = route_ids.shape[1]
    capacity = (5 * tok_rows * pick_count + 4 * expert_count - 1) // (4 * expert_count)
    slot_index = slot_table(route_ids, expert_count, capacity)
    assigned = slot_index.shape[0]
    source = (
        jnp.zeros((expert_count * capacity,), jnp.int32)
        .at[slot_index]
        .set(jnp.arange(assigned, dtype=jnp.int32) // pick_count)
    )
    filled = (
        jnp.zeros((expert_count * capacity,), jnp.bfloat16)
        .at[slot_index]
        .set(jnp.ones((assigned,), jnp.bfloat16))
    )
    gate_local = gate_weight[0]
    up_local = up_weight[0]
    down_local = down_weight[0]
    mixed_share = lax.psum_scatter(
        partial_value.astype(jnp.bfloat16), "tp", scatter_dimension=1, tiled=True
    ).astype(jnp.float32)
    own_width = mixed_share.shape[1]
    col_start = lax.axis_index("tp") * own_width
    own_res = lax.dynamic_slice_in_dim(residual, col_start, own_width, 1).astype(jnp.float32)
    own_cols = (own_res + mixed_share).astype(jnp.bfloat16).astype(jnp.float32)
    square_total = lax.psum(jnp.sum(own_cols * own_cols, axis=1), "tp")
    gain_cols = lax.dynamic_slice_in_dim(norm_gain, col_start, own_width, 0)
    normed_share = (
        own_cols * lax.rsqrt(square_total / model_width + epsilon)[:, None] * gain_cols
    ).astype(jnp.bfloat16)
    outgoing = (normed_share[source] * filled[:, None]).reshape(expert_count, capacity, -1)
    piece = lax.all_gather(
        lax.all_to_all(outgoing, "sp", split_axis=0, concat_axis=0, tiled=True),
        "tp",
        axis=2,
        tiled=True,
    )
    gate_pre = jnp.einsum("scd,df->scf", piece, gate_local, preferred_element_type=jnp.float32)
    up_pre = jnp.einsum("scd,df->scf", piece, up_local, preferred_element_type=jnp.float32)
    hidden = activate(gate_pre, up_pre).astype(jnp.bfloat16)
    share = jnp.einsum("scf,fd->scd", hidden, down_local, preferred_element_type=jnp.float32)
    returned = lax.psum_scatter(share.astype(jnp.bfloat16), "tp", scatter_dimension=2, tiled=True)
    arrived = lax.all_to_all(returned, "sp", split_axis=0, concat_axis=0, tiled=True)
    columns = arrived.shape[2]
    taken_rows = arrived.reshape(expert_count * capacity, columns)[slot_index]
    taken_rows = taken_rows.astype(jnp.float32).reshape(tok_rows, pick_count, columns)
    routed = jnp.sum(taken_rows * route_weights[:, :, None], axis=1)
    return (own_cols + routed).astype(jnp.bfloat16)


def solution(mesh):
    placed = (
        P("sp", None),
        P("sp", "tp"),
        P("sp", "tp"),
        P("sp", "tp"),
        P("tp", "sp"),
        P(),
        P(),
        P("tp", None),
        P(),
        P("sp", None),
        P("sp", None),
        P("sp", None, "tp"),
        P("sp", None, "tp"),
        P("sp", "tp", None),
    )
    return jax.shard_map(
        per_device, mesh=mesh, in_specs=placed, out_specs=P("sp", "tp"), check_vma=False
    )
```

profile of v0, /device:TPU:0, one launch (start us, length us, event | category | flops | bytes accessed | tf_op | source)
XLA Modules:
  0.0 249.5 jit_solution(2540238676448930279)
XLA Ops:
  6.5 1.2 copy.26
  7.8 0.7 mul.146
  8.5 0.8 fusion.52
  9.4 1.7 copy.25
  11.1 1.0 copy.27
  12.1 0.8 copy.29
  13.1 0.6 reduce-window.24
  13.7 28.2 %all_gather.14 = bf16[8,1024]{1,0:T(8,128)(2,1)S(1)} all-gather(bf16[8,128]{1,0:T(8,128)(2,1)} %param.20), channel_id=1, replica_groups=mesh['sp'=8,'tp'=4] {'sp'}, dimensions={1}, use_global_device_ids=true | all-gather | bytes 18432 | tf_op jit(solution)/shard_map/all_gather | solution.py:93
  42.0 0.7 multiply_convert_fusion
  42.7 8.9 %all-gather.6.cloned.1.call-done = bf16[1024,512]{0,1:T(8,128)(2,1)} async-done(((bf16[128,512]{0,1:T(8,128)(2,1)}), bf16[1024,512]{0,1:T(8,128)(2,1)}) %all-gather.6.cloned.1.call-update) | async-done | bytes 1048592 | tf_op jit(solution)/shard_map/all_gather | solution.py:91
  51.6 40.3 %all-gather.4.cloned.1.call-done = bf16[1024,512]{0,1:T(8,128)(2,1)} async-done(((bf16[128,512]{0,1:T(8,128)(2,1)}), bf16[1024,512]{0,1:T(8,128)(2,1)}) %all-gather.4.cloned.1.call-update) | async-done | bytes 1048592 | tf_op jit(solution)/shard_map/all_gather | solution.py:92
  91.9 33.3 %while.16 = (s32[]{:T(128)}, f32[128,8,64]{0,2,1:T(8,128)S(1)}, f32[8,128]{1,0:T(8,128)S(1)}, bf16[1024,512]{0,1:T(8,128)(2,1)}, bf16[1024,512]{0,1:T(8,128)(2,1...) while((s32[]{:T(128)}, f32[128,8,64]{0,2,1:T(8,128)S(1)}, ...), condition=%wide.region_6.7_spmd.clone, body=%wide.region_2.6_spmd.clone.sunk | while | flops 219436672 | bytes 27240652 | solution.py:111
  91.9 1.3 constant_dynamic-slice_fusion.3
  93.2 0.2 compare_and_fusion.2
  93.4 3.0 %fusion.93 = (f32[8,128]{1,0:T(8,128)S(1)}, f32[8,128,512]{1,2,0:T(8,128)S(1)}, f32[8,512,128]{2,1,0:T(8,128)}) fusion(f32[8,512]{1,0:T(8,128)S(1)} %dynamic-slice_convert_fusion.2, pred[128,512]{0,1:T(8,128)(4,1)S(1)} %compare_and_fusion.2, bf16[512,8,64]{0,2,1:T(8,128)(2,1)S(1)} %bitcast.116, bf16[128,8,64]{0,2,1:T(8,128)(2,1)S(1)} %get-tuple-element.292), kind=kOutput, calls=%fused_computation.39.clone.1 | convolution fusion | flops 72875008 | bytes 4935680 | tf_op jit(solution)/shard_map/while/body/eval_jaxpr/qhd,khd->hqk/dot_general | solution.py:42
  96.4 5.0 %fusion.94 = f32[8,128,4,128]{1,0,3,2:T(8,128)S(1)} fusion(f32[8,128,4,128]{1,3,2,0:T(8,128)S(1)} %bitcast.114), kind=kOutput, calls=%fused_computation.23.clone.1 | output fusion | flops 66584576 | bytes 4194304 | tf_op jit(solution)/shard_map/reduce-window.6
  101.6 1.7 copy.38
  103.3 4.8 %fusion.97 = bf16[8,128,512]{1,2,0:T(8,128)(2,1)S(1)} fusion(f32[8,128,4,128]{1,3,2,0:T(8,128)} %copy.38, f32[8,512,128]{2,1,0:T(8,128)} %get-tuple-element.259, f32[8,128]{1,0:T(8,128)S(1)} %get-tuple-element.261, f32[8,512]{1,0:T(8,128)S(1)} %dynamic-slice_convert_fusion.2, pred[128,512]{0,1:T(8,128)(4,1)S(1)} %compare_and_fusion.2), kind=kLoop, calls=%fused_computation.12.clone.1 | loop fusion | flops 12058624 | bytes 5328896 | tf_op jit(solution)/shard_map/while/body/eval_jaxpr/convert_element_type | solution.py:55
  108.1 0.3 fusion.98
  108.5 1.3 constant_dynamic-slice_fusion.3
  109.8 0.2 compare_and_fusion.2
  110.1 3.0 %fusion.93 = (f32[8,128]{1,0:T(8,128)S(1)}, f32[8,128,512]{1,2,0:T(8,128)S(1)}, f32[8,512,128]{2,1,0:T(8,128)}) fusion(f32[8,512]{1,0:T(8,128)S(1)} %dynamic-slice_convert_fusion.2, pred[128,512]{0,1:T(8,128)(4,1)S(1)} %compare_and_fusion.2, bf16[512,8,64]{0,2,1:T(8,128)(2,1)S(1)} %bitcast.116, bf16[128,8,64]{0,2,1:T(8,128)(2,1)S(1)} %get-tuple-element.292), kind=kOutput, calls=%fused_computation.39.clone.1 | convolution fusion | flops 72875008 | bytes 4935680 | tf_op jit(solution)/shard_map/while/body/eval_jaxpr/qhd,khd->hqk/dot_general | solution.py:42
  113.1 5.0 %fusion.94 = f32[8,128,4,128]{1,0,3,2:T(8,128)S(1)} fusion(f32[8,128,4,128]{1,3,2,0:T(8,128)S(1)} %bitcast.114), kind=kOutput, calls=%fused_computation.23.clone.1 | output fusion | flops 66584576 | bytes 4194304 | tf_op jit(solution)/shard_map/reduce-window.6
  118.3 1.7 copy.38
  120.0 4.8 %fusion.97 = bf16[8,128,512]{1,2,0:T(8,128)(2,1)S(1)} fusion(f32[8,128,4,128]{1,3,2,0:T(8,128)} %copy.38, f32[8,512,128]{2,1,0:T(8,128)} %get-tuple-element.259, f32[8,128]{1,0:T(8,128)S(1)} %get-tuple-element.261, f32[8,512]{1,0:T(8,128)S(1)} %dynamic-slice_convert_fusion.2, pred[128,512]{0,1:T(8,128)(4,1)S(1)} %compare_and_fusion.2), kind=kLoop, calls=%fused_computation.12.clone.1 | loop fusion | flops 12058624 | bytes 5328896 | tf_op jit(solution)/shard_map/while/body/eval_jaxpr/convert_element_type | solution.py:55
  124.8 0.3 fusion.98
  125.2 2.9 %convolution_convert_fusion.1 = bf16[128,2048]{1,0:T(8,128)(2,1)} fusion(bf16[128,512]{0,1:T(8,128)(2,1)S(1)} %bitcast.118, bf16[512,2048]{1,0:T(8,128)(2,1)} %param.23), kind=kOutput, calls=%fused_computation.41 | convolution fusion | flops 268697600 | bytes 2752512 | tf_op jit(solution)/shard_map/dot_general | solution.py:113
  128.1 0.2 slice_reduce_fusion
  128.3 0.1 eq.25
  128.9 1.4 scatter_custom_fusion
  130.3 2.2 scatter_custom_fusion.1
  132.6 0.8 dynamic_slice.28
  133.3 15.6 %reduce-scatter.3.cloned.1.call-done = bf16[128,512]{1,0:T(8,128)(2,1)} async-done(((bf16[128,2048]{1,0:T(8,128)(2,1)}), bf16[128,512]{1,0:T(8,128)(2,1)}) %reduce-scatter.3.cloned.1.call-update) | async-done | bytes 131088 | tf_op jit(solution)/shard_map/reduce_scatter | solution.py:133
  148.9 1.1 fusion.53
  150.0 5.8 %psum.7 = f32[128]{0:T(128)S(1)} all-reduce(f32[128]{0:T(128)S(1)} %get-tuple-element.193), channel_id=1, replica_groups=mesh['sp'=8,'tp'=4] {'tp'}, use_global_device_ids=true, to_apply=%region_9.10 | all-reduce | flops 128 | bytes 1024 | tf_op jit(solution)/shard_map/psum | solution.py:140
  155.9 2.0 gather_fusion
  158.0 16.3 %all_to_all.10 = bf16[8,40,512]{2,1,0:T(8,128)(2,1)} all-to-all(bf16[8,40,512]{2,1,0:T(8,128)(2,1)S(1)} %broadcast_multiply_fusion), channel_id=1, replica_groups=mesh['sp'=8,'tp'=4] {'sp'}, dimensions={0} | all-to-all | bytes 655360 | tf_op jit(solution)/shard_map/all_to_all | solution.py:147
  174.4 0.2 reduce-scatter.5.cloned.1.call-start
  174.6 15.6 %all-gather.8.cloned.1.call-done = bf16[8,40,2048]{2,1,0:T(8,128)(2,1)} async-done(((bf16[8,40,512]{2,1,0:T(8,128)(2,1)}), bf16[8,40,2048]{2,1,0:T(8,128)(2,1)}) %all-gather.8.cloned.1.call-update) | async-done | bytes 1310736 | tf_op jit(solution)/shard_map/all_gather | solution.py:146
  190.1 2.8 %fusion.33 = f32[8,40,512]{2,1,0:T(8,128)S(1)} fusion(bf16[8,40,2048]{2,1,0:T(8,128)(2,1)} %all-gather.8.cloned.1.call-done, bf16[1,2048,512]{2,1,0:T(8,128)(2,1)} %param.27), kind=kOutput, calls=%fused_computation.50 | convolution fusion | flops 671252480 | bytes 4063232 | tf_op jit(solution)/shard_map/scd,df->scf/dot_general | solution.py:152
  193.0 4.8 %convolution_convert_fusion = bf16[8,40,2048]{2,1,0:T(8,128)(2,1)} fusion(bf16[1,512,2048]{2,1,0:T(8,128)(2,1)S(1)} %copy-done, bf16[8,40,2048]{2,1,0:T(8,128)(2,1)} %all-gather.8.cloned.1.call-done, bf16[1,2048,512]{2,1,0:T(8,128)(2,1)} %param.28, f32[8,40,512]{2,1,0:T(8,128)S(1)} %fusion.33), kind=kOutput, calls=%fused_computation.40 | convolution fusion | flops 1344307200 | bytes 7471104 | tf_op jit(solution)/shard_map/scf,fd->scd/dot_general | solution.py:155
  197.8 26.6 %reduce-scatter.5.cloned.1.call-done = bf16[8,40,512]{2,1,0:T(8,128)(2,1)} async-done(((bf16[8,40,2048]{2,1,0:T(8,128)(2,1)}), bf16[8,40,512]{2,1,0:T(8,128)(2,1)}) %reduce-scatter.5.cloned.1.call-update) | async-done | bytes 327696 | tf_op jit(solution)/shard_map/reduce_scatter | solution.py:156
  224.4 5.5 %all-to-all-start.1 = ((bf16[8,40,512]{2,1,0:T(8,128)(2,1)}), bf16[8,40,512]{2,1,0:T(8,128)(2,1)S(1)}, u32[]{:S(2)}, u32[]{:S(2)}) async-start(bf16[8,40,512]{2,1,0:T(8,128)(2,1)} %reduce-scatter.5.cloned.1.call-done), calls=%async_computation.3 | async-start | bytes 655360 | tf_op jit(solution)/shard_map/all_to_all | solution.py:157
  230.0 10.0 %all-to-all-done.1 = bf16[8,40,512]{2,1,0:T(8,128)(2,1)S(1)} async-done(((bf16[8,40,512]{2,1,0:T(8,128)(2,1)}), bf16[8,40,512]{2,1,0:T(8,128)(2,1)S(1)}, u32[]{:S(2)}, u32[]{:S(2)}) %all-to-all-start.1) | async-done | bytes 327712 | tf_op jit(solution)/shard_map/all_to_all | solution.py:157
  240.1 1.2 gather_fusion.1
  241.2 0.3 reshape.188
  241.5 0.7 multiply_reduce_fusion
  242.3 0.7 fusion.56
  (58 shorter events, 1.8 us)
Async XLA Ops:
  6.5 186.5 %copy-start = (bf16[1,512,2048]{2,1,0:T(8,128)(2,1)S(1)}, bf16[1,512,2048]{2,1,0:T(8,128)(2,1)}, u32[]{:S(2)}) copy-start(bf16[1,512,2048]{2,1,0:T(8,128)(2,1)} %param.29) | copy-start | bytes 6291460
  6.5 45.1 %all-gather.6.cloned.1.call-start = ((), (), s32[]{:S(2)}) async-start(), calls=%async_computation.5 | async-start | bytes 1179648 | tf_op jit(solution)/shard_map/all_gather | solution.py:91
  9.3 82.6 %all-gather.4.cloned.1.call-start = ((), (), s32[]{:S(2)}) async-start(), calls=%async_computation.4 | async-start | bytes 1179648 | tf_op jit(solution)/shard_map/all_gather | solution.py:92
  11.1 137.9 %reduce-scatter.3.cloned.1.call-start = ((), (), s32[]{:S(2)}) async-start(), calls=%async_computation.6 | async-start | bytes 655360 | tf_op jit(solution)/shard_map/reduce_scatter | solution.py:133
  125.1 3.4 %copy-start.1 = (s32[128,2]{0,1:T(2,128)S(1)}, s32[128,2]{0,1:T(2,128)}, u32[]{:S(2)}) copy-start(s32[128,2]{0,1:T(2,128)} %param.25) | copy-start | bytes 3076
  128.1 62.1 %all-gather.8.cloned.1.call-start = ((), (), s32[]{:S(2)}) async-start(), calls=%async_computation.7 | async-start | bytes 1638400 | tf_op jit(solution)/shard_map/all_gather | solution.py:146
  174.4 50.0 %reduce-scatter.5.cloned.1.call-start = ((), (), s32[]{:S(2)}) async-start(), calls=%async_computation.8 | async-start | bytes 1638400 | tf_op jit(solution)/shard_map/reduce_scatter | solution.py:156
  193.0 36.9 %copy-start.2 = (f32[128,2]{0,1:T(2,128)S(1)}, f32[128,2]{0,1:T(2,128)}, u32[]{:S(2)}) copy-start(f32[128,2]{0,1:T(2,128)} %param.26) | copy-start | bytes 3076
  224.4 15.7 %all-to-all-start.1 = ((bf16[8,40,512]{2,1,0:T(8,128)(2,1)}), bf16[8,40,512]{2,1,0:T(8,128)(2,1)S(1)}, u32[]{:S(2)}, u32[]{:S(2)}) async-start(bf16[8,40,512]{2,1,0:T(8,128)(2,1)} %reduce-scatter.5.cloned.1.call-done), calls=%async_computation.3 | async-start | bytes 655360 | tf_op jit(solution)/shard_map/all_to_all | solution.py:157
Sparse Core Ops, SparseCore 0:
  9.4 42.1 all-gather.5
  53.6 38.1 all-gather.3
  128.2 20.6 reduce-scatter.2
  174.5 15.6 all-gather.7
  197.9 26.4 reduce-scatter.4
where the time goes:
time: 250 us; the launch traced here: 249 us
  waiting for transfers between devices  117 us (47%)
  blocking collectives  50.3 us (20%)
  other arithmetic  25.5 us (10%)
  local copies, waits for them, and re-layouts  20.1 us (8%)
  matrix products  17.2 us (7%)
  between operations  13.4 us (5%)
  starting transfers between devices  5.86 us (2%)
    all_gather x1, waiting for transfers between devices, per_device(): lax.all_gather(values, 'sp', axis=0, tiled=True)  40.3 us
    all_gather x1, blocking collectives, per_device(): lax.all_gather(stick_bias, 'sp', axis=1, tiled=True)  28.2 us
    reduce_scatter x1, waiting for transfers between devices, per_device(): lax.psum_scatter(share.astype(jnp.bfloat16), 'tp', scatter_dimension=2, t...  26.6 us
    all_to_all x1, blocking collectives, per_device(): lax.all_to_all(outgoing, 'sp', split_axis=0, concat_axis=0, tiled=True)  16.3 us
    reduce_scatter x1, waiting for transfers between devices, per_device(): lax.psum_scatter(partial_value.astype(jnp.bfloat16), 'tp', scatter_dimens...  15.6 us
    all_gather x1, waiting for transfers between devices, per_device(): lax.all_gather(lax.all_to_all(outgoing, 'sp', split_axis=0, concat_axis=0...  15.6 us
    another operation x6, other arithmetic  10.7 us
    all_to_all x1, waiting for transfers between devices, per_device(): lax.all_to_all(returned, 'sp', split_axis=0, concat_axis=0, tiled=True)  10 us
  transfers between devices with their start and end apart: 6, of which 6 were waited for; matrix products, arithmetic and copies ran while one was open for 4% of the time, Pallas kernels for 0%

commit v1 on v0

--- a/solution.py
+++ b/solution.py
@@ -7,6 +7,10 @@
 epsilon = 1e-06
 clamp_limit = 7.0
 swish_scale = 1.702
+
+
+def get_ports(shard_in, dim_i):
+    return jnp.concatenate(lax.all_gather(shard_in, axis_name="sp"), dim_i)
 
 
 def head_normalize(packed, gain):
@@ -90,7 +94,7 @@
     all_keys, all_values, all_bias = (
         lax.all_gather(keys_n, "sp", axis=0, tiled=True),
         lax.all_gather(values, "sp", axis=0, tiled=True),
-        lax.all_gather(stick_bias, "sp", axis=1, tiled=True),
+        get_ports(stick_bias, 1),
     )
     key_total = all_keys.shape[0]
     block_len = math.gcd(key_total, 512)

time: 250 us -> 250 us (level)
  no operation moved by 1% of the time
where the time goes in v1:
time: 250 us; the launch traced here: 249 us
  waiting for transfers between devices  117 us (47%)
  blocking collectives  50.3 us (20%)
  other arithmetic  25.5 us (10%)
  local copies, waits for them, and re-layouts  20.1 us (8%)
  matrix products  17.2 us (7%)
  between operations  13.4 us (5%)
  starting transfers between devices  5.86 us (2%)
    all_gather x1, waiting for transfers between devices, per_device(): lax.all_gather(values, 'sp', axis=0, tiled=True)  40.3 us
    all_gather x1, blocking collectives, get_ports(): return jnp.concatenate(lax.all_gather(shard_in, axis_name='sp'), dim_i)  28.2 us
    reduce_scatter x1, waiting for transfers between devices, per_device(): lax.psum_scatter(share.astype(jnp.bfloat16), 'tp', scatter_dimension=2, t...  26.6 us
    all_to_all x1, blocking collectives, per_device(): lax.all_to_all(outgoing, 'sp', split_axis=0, concat_axis=0, tiled=True)  16.3 us
    reduce_scatter x1, waiting for transfers between devices, per_device(): lax.psum_scatter(partial_value.astype(jnp.bfloat16), 'tp', scatter_dimens...  15.6 us
    all_gather x1, waiting for transfers between devices, per_device(): lax.all_gather(lax.all_to_all(outgoing, 'sp', split_axis=0, concat_axis=0...  15.6 us
    another operation x6, other arithmetic  10.7 us
    all_to_all x1, waiting for transfers between devices, per_device(): lax.all_to_all(returned, 'sp', split_axis=0, concat_axis=0, tiled=True)  10 us
  transfers between devices with their start and end apart: 6, of which 6 were waited for; matrix products, arithmetic and copies ran while one was open for 4% of the time, Pallas kernels for 0%

profile of v1, /device:TPU:0, one launch (start us, length us, event | category | flops | bytes accessed | tf_op | source)
XLA Modules:
  0.0 249.5 jit_solution(15424628666111324970)
XLA Ops:
  6.5 1.2 copy.26
  7.8 0.7 mul.146
  8.5 0.8 fusion.52
  9.4 1.7 copy.25
  11.1 1.0 copy.27
  12.1 0.8 copy.29
  13.1 0.6 reduce-window.24
  13.7 28.2 %all-gather = bf16[64,128]{1,0:T(8,128)(2,1)S(1)} all-gather(bf16[8,128]{1,0:T(8,128)(2,1)} %param.20), channel_id=2, replica_groups=mesh['sp'=8,'tp'=4] {'sp'}, dimensions={0}, use_global_device_ids=true | all-gather | bytes 18432 | tf_op jit(solution)/shard_map/all_gather | solution.py:13
  42.0 0.7 multiply_convert_fusion
  42.7 8.9 %all-gather.7.cloned.1.call-done = bf16[1024,512]{0,1:T(8,128)(2,1)} async-done(((bf16[128,512]{0,1:T(8,128)(2,1)}), bf16[1024,512]{0,1:T(8,128)(2,1)}) %all-gather.7.cloned.1.call-update) | async-done | bytes 1048592 | tf_op jit(solution)/shard_map/all_gather | solution.py:95
  51.6 40.3 %all-gather.5.cloned.1.call-done = bf16[1024,512]{0,1:T(8,128)(2,1)} async-done(((bf16[128,512]{0,1:T(8,128)(2,1)}), bf16[1024,512]{0,1:T(8,128)(2,1)}) %all-gather.5.cloned.1.call-update) | async-done | bytes 1048592 | tf_op jit(solution)/shard_map/all_gather | solution.py:96
  91.9 33.3 %while.16 = (s32[]{:T(128)}, f32[128,8,64]{0,2,1:T(8,128)S(1)}, f32[8,128]{1,0:T(8,128)S(1)}, bf16[1024,512]{0,1:T(8,128)(2,1)}, bf16[1024,512]{0,1:T(8,128)(2,1...) while((s32[]{:T(128)}, f32[128,8,64]{0,2,1:T(8,128)S(1)}, ...), condition=%wide.region_6.7_spmd.clone, body=%wide.region_2.6_spmd.clone.sunk | while | flops 219436672 | bytes 27240652 | solution.py:115
  91.9 1.3 constant_dynamic-slice_fusion.3
  93.2 0.2 compare_and_fusion.2
  93.4 3.0 %fusion.93 = (f32[8,128]{1,0:T(8,128)S(1)}, f32[8,128,512]{1,2,0:T(8,128)S(1)}, f32[8,512,128]{2,1,0:T(8,128)}) fusion(f32[8,512]{1,0:T(8,128)S(1)} %dynamic-slice_convert_fusion.2, pred[128,512]{0,1:T(8,128)(4,1)S(1)} %compare_and_fusion.2, bf16[512,8,64]{0,2,1:T(8,128)(2,1)S(1)} %bitcast.121, bf16[128,8,64]{0,2,1:T(8,128)(2,1)S(1)} %get-tuple-element.292), kind=kOutput, calls=%fused_computation.39.clone.1 | convolution fusion | flops 72875008 | bytes 4935680 | tf_op jit(solution)/shard_map/while/body/eval_jaxpr/qhd,khd->hqk/dot_general | solution.py:46
  96.4 5.0 %fusion.94 = f32[8,128,4,128]{1,0,3,2:T(8,128)S(1)} fusion(f32[8,128,4,128]{1,3,2,0:T(8,128)S(1)} %bitcast.119), kind=kOutput, calls=%fused_computation.23.clone.1 | output fusion | flops 66584576 | bytes 4194304 | tf_op jit(solution)/shard_map/reduce-window.6
  101.6 1.7 copy.38
  103.3 4.8 %fusion.97 = bf16[8,128,512]{1,2,0:T(8,128)(2,1)S(1)} fusion(f32[8,128,4,128]{1,3,2,0:T(8,128)} %copy.38, f32[8,512,128]{2,1,0:T(8,128)} %get-tuple-element.259, f32[8,128]{1,0:T(8,128)S(1)} %get-tuple-element.261, f32[8,512]{1,0:T(8,128)S(1)} %dynamic-slice_convert_fusion.2, pred[128,512]{0,1:T(8,128)(4,1)S(1)} %compare_and_fusion.2), kind=kLoop, calls=%fused_computation.12.clone.1 | loop fusion | flops 12058624 | bytes 5328896 | tf_op jit(solution)/shard_map/while/body/eval_jaxpr/convert_element_type | solution.py:59
  108.1 0.3 fusion.98
  108.5 1.3 constant_dynamic-slice_fusion.3
  109.8 0.2 compare_and_fusion.2
  110.1 3.0 %fusion.93 = (f32[8,128]{1,0:T(8,128)S(1)}, f32[8,128,512]{1,2,0:T(8,128)S(1)}, f32[8,512,128]{2,1,0:T(8,128)}) fusion(f32[8,512]{1,0:T(8,128)S(1)} %dynamic-slice_convert_fusion.2, pred[128,512]{0,1:T(8,128)(4,1)S(1)} %compare_and_fusion.2, bf16[512,8,64]{0,2,1:T(8,128)(2,1)S(1)} %bitcast.121, bf16[128,8,64]{0,2,1:T(8,128)(2,1)S(1)} %get-tuple-element.292), kind=kOutput, calls=%fused_computation.39.clone.1 | convolution fusion | flops 72875008 | bytes 4935680 | tf_op jit(solution)/shard_map/while/body/eval_jaxpr/qhd,khd->hqk/dot_general | solution.py:46
  113.1 5.0 %fusion.94 = f32[8,128,4,128]{1,0,3,2:T(8,128)S(1)} fusion(f32[8,128,4,128]{1,3,2,0:T(8,128)S(1)} %bitcast.119), kind=kOutput, calls=%fused_computation.23.clone.1 | output fusion | flops 66584576 | bytes 4194304 | tf_op jit(solution)/shard_map/reduce-window.6
  118.3 1.7 copy.38
  120.0 4.8 %fusion.97 = bf16[8,128,512]{1,2,0:T(8,128)(2,1)S(1)} fusion(f32[8,128,4,128]{1,3,2,0:T(8,128)} %copy.38, f32[8,512,128]{2,1,0:T(8,128)} %get-tuple-element.259, f32[8,128]{1,0:T(8,128)S(1)} %get-tuple-element.261, f32[8,512]{1,0:T(8,128)S(1)} %dynamic-slice_convert_fusion.2, pred[128,512]{0,1:T(8,128)(4,1)S(1)} %compare_and_fusion.2), kind=kLoop, calls=%fused_computation.12.clone.1 | loop fusion | flops 12058624 | bytes 5328896 | tf_op jit(solution)/shard_map/while/body/eval_jaxpr/convert_element_type | solution.py:59
  124.8 0.3 fusion.98
  125.2 2.9 %convolution_convert_fusion.1 = bf16[128,2048]{1,0:T(8,128)(2,1)} fusion(bf16[128,512]{0,1:T(8,128)(2,1)S(1)} %bitcast.123, bf16[512,2048]{1,0:T(8,128)(2,1)} %param.23), kind=kOutput, calls=%fused_computation.41 | convolution fusion | flops 268697600 | bytes 2752512 | tf_op jit(solution)/shard_map/dot_general | solution.py:117
  128.1 0.2 slice_reduce_fusion
  128.3 0.1 eq.25
  128.9 1.4 scatter_custom_fusion
  130.3 2.2 scatter_custom_fusion.1
  132.6 0.8 dynamic_slice.28
  133.3 15.6 %reduce-scatter.3.cloned.1.call-done = bf16[128,512]{1,0:T(8,128)(2,1)} async-done(((bf16[128,2048]{1,0:T(8,128)(2,1)}), bf16[128,512]{1,0:T(8,128)(2,1)}) %reduce-scatter.3.cloned.1.call-update) | async-done | bytes 131088 | tf_op jit(solution)/shard_map/reduce_scatter | solution.py:137
  148.9 1.1 fusion.53
  150.0 5.8 %psum.7 = f32[128]{0:T(128)S(1)} all-reduce(f32[128]{0:T(128)S(1)} %get-tuple-element.193), channel_id=1, replica_groups=mesh['sp'=8,'tp'=4] {'tp'}, use_global_device_ids=true, to_apply=%region_9.10 | all-reduce | flops 128 | bytes 1024 | tf_op jit(solution)/shard_map/psum | solution.py:144
  155.9 2.0 gather_fusion
  158.0 16.3 %all_to_all.10 = bf16[8,40,512]{2,1,0:T(8,128)(2,1)} all-to-all(bf16[8,40,512]{2,1,0:T(8,128)(2,1)S(1)} %broadcast_multiply_fusion), channel_id=1, replica_groups=mesh['sp'=8,'tp'=4] {'sp'}, dimensions={0} | all-to-all | bytes 655360 | tf_op jit(solution)/shard_map/all_to_all | solution.py:151
  174.4 0.2 reduce-scatter.5.cloned.1.call-start
  174.6 15.6 %all-gather.9.cloned.1.call-done = bf16[8,40,2048]{2,1,0:T(8,128)(2,1)} async-done(((bf16[8,40,512]{2,1,0:T(8,128)(2,1)}), bf16[8,40,2048]{2,1,0:T(8,128)(2,1)}) %all-gather.9.cloned.1.call-update) | async-done | bytes 1310736 | tf_op jit(solution)/shard_map/all_gather | solution.py:150
  190.1 2.8 %fusion.33 = f32[8,40,512]{2,1,0:T(8,128)S(1)} fusion(bf16[8,40,2048]{2,1,0:T(8,128)(2,1)} %all-gather.9.cloned.1.call-done, bf16[1,2048,512]{2,1,0:T(8,128)(2,1)} %param.27), kind=kOutput, calls=%fused_computation.50 | convolution fusion | flops 671252480 | bytes 4063232 | tf_op jit(solution)/shard_map/scd,df->scf/dot_general | solution.py:156
  193.0 4.8 %convolution_convert_fusion = bf16[8,40,2048]{2,1,0:T(8,128)(2,1)} fusion(bf16[1,512,2048]{2,1,0:T(8,128)(2,1)S(1)} %copy-done, bf16[8,40,2048]{2,1,0:T(8,128)(2,1)} %all-gather.9.cloned.1.call-done, bf16[1,2048,512]{2,1,0:T(8,128)(2,1)} %param.28, f32[8,40,512]{2,1,0:T(8,128)S(1)} %fusion.33), kind=kOutput, calls=%fused_computation.40 | convolution fusion | flops 1344307200 | bytes 7471104 | tf_op jit(solution)/shard_map/scf,fd->scd/dot_general | solution.py:159
  197.8 26.6 %reduce-scatter.5.cloned.1.call-done = bf16[8,40,512]{2,1,0:T(8,128)(2,1)} async-done(((bf16[8,40,2048]{2,1,0:T(8,128)(2,1)}), bf16[8,40,512]{2,1,0:T(8,128)(2,1)}) %reduce-scatter.5.cloned.1.call-update) | async-done | bytes 327696 | tf_op jit(solution)/shard_map/reduce_scatter | solution.py:160
  224.4 5.5 %all-to-all-start.1 = ((bf16[8,40,512]{2,1,0:T(8,128)(2,1)}), bf16[8,40,512]{2,1,0:T(8,128)(2,1)S(1)}, u32[]{:S(2)}, u32[]{:S(2)}) async-start(bf16[8,40,512]{2,1,0:T(8,128)(2,1)} %reduce-scatter.5.cloned.1.call-done), calls=%async_computation.3 | async-start | bytes 655360 | tf_op jit(solution)/shard_map/all_to_all | solution.py:161
  230.0 10.0 %all-to-all-done.1 = bf16[8,40,512]{2,1,0:T(8,128)(2,1)S(1)} async-done(((bf16[8,40,512]{2,1,0:T(8,128)(2,1)}), bf16[8,40,512]{2,1,0:T(8,128)(2,1)S(1)}, u32[]{:S(2)}, u32[]{:S(2)}) %all-to-all-start.1) | async-done | bytes 327712 | tf_op jit(solution)/shard_map/all_to_all | solution.py:161
  240.1 1.2 gather_fusion.1
  241.2 0.3 reshape.196
  241.5 0.7 multiply_reduce_fusion
  242.3 0.7 fusion.56
  (58 shorter events, 1.8 us)
Async XLA Ops:
  6.5 186.5 %copy-start = (bf16[1,512,2048]{2,1,0:T(8,128)(2,1)S(1)}, bf16[1,512,2048]{2,1,0:T(8,128)(2,1)}, u32[]{:S(2)}) copy-start(bf16[1,512,2048]{2,1,0:T(8,128)(2,1)} %param.29) | copy-start | bytes 6291460
  6.5 45.1 %all-gather.7.cloned.1.call-start = ((), (), s32[]{:S(2)}) async-start(), calls=%async_computation.5 | async-start | bytes 1179648 | tf_op jit(solution)/shard_map/all_gather | solution.py:95
  9.3 82.6 %all-gather.5.cloned.1.call-start = ((), (), s32[]{:S(2)}) async-start(), calls=%async_computation.4 | async-start | bytes 1179648 | tf_op jit(solution)/shard_map/all_gather | solution.py:96
  11.1 137.9 %reduce-scatter.3.cloned.1.call-start = ((), (), s32[]{:S(2)}) async-start(), calls=%async_computation.6 | async-start | bytes 655360 | tf_op jit(solution)/shard_map/reduce_scatter | solution.py:137
  125.1 3.4 %copy-start.1 = (s32[128,2]{0,1:T(2,128)S(1)}, s32[128,2]{0,1:T(2,128)}, u32[]{:S(2)}) copy-start(s32[128,2]{0,1:T(2,128)} %param.25) | copy-start | bytes 3076
  128.1 62.1 %all-gather.9.cloned.1.call-start = ((), (), s32[]{:S(2)}) async-start(), calls=%async_computation.7 | async-start | bytes 1638400 | tf_op jit(solution)/shard_map/all_gather | solution.py:150
  174.4 50.0 %reduce-scatter.5.cloned.1.call-start = ((), (), s32[]{:S(2)}) async-start(), calls=%async_computation.8 | async-start | bytes 1638400 | tf_op jit(solution)/shard_map/reduce_scatter | solution.py:160
  193.0 36.9 %copy-start.2 = (f32[128,2]{0,1:T(2,128)S(1)}, f32[128,2]{0,1:T(2,128)}, u32[]{:S(2)}) copy-start(f32[128,2]{0,1:T(2,128)} %param.26) | copy-start | bytes 3076
  224.4 15.7 %all-to-all-start.1 = ((bf16[8,40,512]{2,1,0:T(8,128)(2,1)}), bf16[8,40,512]{2,1,0:T(8,128)(2,1)S(1)}, u32[]{:S(2)}, u32[]{:S(2)}) async-start(bf16[8,40,512]{2,1,0:T(8,128)(2,1)} %reduce-scatter.5.cloned.1.call-done), calls=%async_computation.3 | async-start | bytes 655360 | tf_op jit(solution)/shard_map/all_to_all | solution.py:161
Sparse Core Ops, SparseCore 0:
  9.4 42.1 all-gather.6
  53.6 38.1 all-gather.4
  128.2 20.6 reduce-scatter.2
  174.5 15.6 all-gather.8
  197.9 26.4 reduce-scatter.4
